TPU v7x, 512 devices: a 8x2x16 block of a 8x8x16 slice. The times are simulated.
512 devices in a mesh: grp: 2 (over y), ep: 32 (over z, core), tp: 8 (over x).
Axes of the slice: x: 8, y: 2, z: 16, core: 2. Of those that a mesh axis runs over, the one named last changes fastest.
The devices are a block of a 8x8x16 slice.
Arguments:
- tokens: bfloat16 [16384, 2048], P(('grp', 'ep'), 'tp'), parts along dimension 0, may hold values from -6 to 6
- norm_gain: float32 [2048], replicated, may hold values from 0.1 to 1.9
- expert_ids: int32 [16384, 2], P(('grp', 'ep')), parts along dimension 0, may hold values from 0 to 31, all different within a row; in each aligned block of 256 rows (0 to 255, 256 to 511, ...) at most 24 rows name the same one
- gate_weights: float32 [16384, 2], P(('grp', 'ep')), parts along dimension 0, may hold values from 0.25 to 1
- w_gate: bfloat16 [32, 2048, 3072], P('ep', None, 'tp'), may hold values from -0.125 to 0.125
- w_up: bfloat16 [32, 2048, 3072], P('ep', None, 'tp'), may hold values from -0.125 to 0.125
- w_down: bfloat16 [32, 3072, 2048], P('ep', 'tp'), may hold values from -0.15625 to 0.15625
Outputs:
- mixed: bfloat16 [16384, 2048], P(('grp', 'ep'), 'tp'), parts along dimension 0
There are 2 independent parts, one for each index of `grp`. A program takes and returns all parts, laid end to end along the dimension named above; an argument that names none is the same for every part. Nothing has to cross between parts.
Inputs may be any that keep to these rules, and one draw needn't show every extreme that they name: `expert_ids`: each token names 2 different experts. Within the 256 rows of one index of ep (aligned blocks) no expert is named more than 24 times, and in some blocks one expert is named exactly 24 times.
All inputs are finite; a program needn't handle non-finite values.
Results may differ from a plain program's by a relative error of at most 0.015.
Values may be sent and summed in bfloat16 or wider, within the bound.
A program may use at most 64 MiB of HBM per device.

v0:
```python
import jax
import jax.numpy as jnp
from jax import lax
from jax.sharding import Mesh
from jax.sharding import PartitionSpec as P

EP = ("ep_0", "ep_1")
GRP_EP = ("grp", "ep_0", "ep_1")


epsilon = 1e-06


def sent_to_all(array, axis):
    count = lax.axis_size(axis)
    return lax.all_to_all(
        jnp.broadcast_to(array[None], (count, *array.shape)), axis, 0, 0, tiled=True
    )


def over_copies(array, axis):
    everything = sent_to_all(array, axis)
    return jnp.sum(everything, axis=0)


def in_blocks(array, dim, count):
    dims = array.shape
    blocks = array.reshape(*dims[:dim], count, dims[dim] // count, *dims[dim + 1 :])
    return jnp.moveaxis(blocks, dim, 0)


def joined_along(blocks, dim):
    dims = list(blocks.shape[1:])
    dims[dim] *= blocks.shape[0]
    return jnp.moveaxis(blocks, 0, dim).reshape(dims)


def moved_by_axis(blocks, axes, order):
    inside = blocks.shape[1:]
    whole = blocks.reshape(*(lax.axis_size(a) for a in axes), *inside)
    for k in order:
        whole = lax.all_to_all(whole, axes[k], k, k, tiled=True)
    return whole.reshape(-1, *inside)


def core_and_chips(array, groups, order, split_dim, concat_dim):
    count = lax.axis_size(groups[0]) * lax.axis_size(groups[1])
    blocks = in_blocks(array, split_dim, count)
    return joined_along(moved_by_axis(blocks, groups, order), concat_dim)


def on_device(tokens, norm_gain, expert_ids, gate_weights, w_gate, w_up, w_down):
    tok_count = tokens.shape[0]
    top_count = expert_ids.shape[1]
    expert_count = lax.axis_size(EP)
    capacity = 3 * tok_count * top_count // (2 * expert_count)
    model_width = norm_gain.shape[0]
    flat_ids = expert_ids.reshape(-1)
    onehot = (flat_ids[:, None] == jnp.arange(expert_count, dtype=jnp.int32)[None, :]).astype(
        jnp.int32
    )
    earlier = jnp.cumsum(onehot, axis=0) - onehot
    slot_index = jnp.sum(earlier * onehot, axis=1)
    dest_index = flat_ids * capacity + slot_index
    owner_index = jnp.arange(tok_count * top_count, dtype=jnp.int32) // top_count
    slot_token = (
        jnp.full((expert_count * capacity,), tok_count, jnp.int32).at[dest_index].set(owner_index)
    )
    tok_values = tokens.astype(jnp.float32)
    square_sum = over_copies(jnp.sum(tok_values * tok_values, axis=1, keepdims=True), "tp")
    col_count = tokens.shape[1]
    gain_part = lax.dynamic_slice_in_dim(norm_gain, lax.axis_index("tp") * col_count, col_count)
    normed = (tok_values * lax.rsqrt(square_sum / model_width + epsilon) * gain_part).astype(
        jnp.bfloat16
    )
    buffer = jnp.take(normed, slot_token, axis=0, mode="fill", fill_value=0).reshape(
        expert_count, capacity, -1
    )
    received = core_and_chips(buffer, ("ep_0", "ep_1"), (1, 0), 0, 0)
    source_count, item_count, col_count = received.shape
    tok_rows = received.reshape(-1, col_count)
    col_piece = lax.all_gather(tok_rows, "tp", axis=1, tiled=True)
    gate_rows = w_gate[0]
    up_rows = w_up[0]
    gate_part = jnp.dot(col_piece, gate_rows, preferred_element_type=jnp.float32)
    up_part = jnp.dot(col_piece, up_rows, preferred_element_type=jnp.float32)
    hidden = (jax.nn.silu(gate_part) * up_part).astype(jnp.bfloat16)
    partial_value = jnp.dot(hidden, w_down[0], preferred_element_type=jnp.float32)
    partial_value = partial_value.reshape(source_count, item_count, -1)
    summed = lax.psum_scatter(
        partial_value.astype(jnp.bfloat16), "tp", scatter_dimension=2, tiled=True
    )
    came_back = lax.all_to_all(summed, EP, split_axis=0, concat_axis=0, tiled=True)
    picked = came_back.reshape(expert_count * capacity, -1)[dest_index].astype(jnp.float32)
    weighted = picked * gate_weights.reshape(-1)[:, None]
    return jnp.sum(weighted.reshape(tok_count, top_count, -1), axis=1).astype(jnp.bfloat16)


def solution(mesh):
    finer = Mesh(
        mesh.devices.reshape(mesh.shape["grp"], 16, 2, mesh.shape["tp"]),
        ("grp", "ep_0", "ep_1", "tp"),
    )
    in_specs = (
        P(GRP_EP, "tp"),
        P(),
        P(GRP_EP, None),
        P(GRP_EP, None),
        P(EP, None, "tp"),
        P(EP, None, "tp"),
        P(EP, "tp", None),
    )
    out_specs = P(GRP_EP, "tp")
    return jax.shard_map(
        on_device, mesh=finer, in_specs=in_specs, out_specs=out_specs, check_vma=False
    )
```

profile of v0, /device:TPU:65, one launch (start us, length us, event | category | flops | bytes accessed | tf_op | source)
XLA Modules:
  0.0 271.2 jit_solution(14151282188558710371)
XLA Ops:
  6.6 1.1 fusion.11
  7.7 0.6 broadcast_in_dim.29
  8.3 7.9 %all-to-all-start = ((f32[8,256,1]{1,2,0:T(1,128)}), f32[8,256,1]{1,2,0:T(1,128)S(1)}, u32[]{:S(2)}, u32[]{:S(2)}) async-start(f32[8,256,1]{1,2,0:T(1,128)} %broadcast_in_dim.29), calls=%async_computation | async-start | bytes 16384 | tf_op jit(solution)/shard_map/all_to_all | solution.py:16
  16.2 0.8 copy.15
  17.0 0.1 eq.29
  17.2 0.1 eq.25
  17.3 0.7 broadcast_multiply_fusion
  18.0 1.2 reduce-window.6
  19.2 0.2 slice_reduce_fusion
  19.5 0.1 copy.14
  19.6 0.1 mul.59
  19.8 0.1 fusion.16
  19.9 2.4 scatter_custom_fusion
  22.4 0.1 broadcast_in_dim.27
  22.5 0.8 dynamic_slice.3
  23.3 1.0 fusion.13
  24.3 2.7 gather_fusion
  27.0 0.2 copy_select_fusion
  27.2 41.3 %all_to_all.20 = bf16[16,2,1,24,256]{4,3,0,2,1:T(8,128)(2,1)S(1)} all-to-all(bf16[16,2,1,24,256]{4,3,0,2,1:T(8,128)(2,1)S(1)} %copy_select_fusion), channel_id=1, replica_groups=mesh['grp'=2,'ep_0'=16,'ep_1'=2,'tp'=8] {'ep_1'}, dimensions={1} | all-to-all | bytes 786432 | tf_op jit(solution)/shard_map/all_to_all | solution.py:42
  68.5 24.6 %all_to_all.21 = bf16[16,2,1,24,256]{4,3,1,2,0:T(8,128)(2,1)} all-to-all(bf16[16,2,1,24,256]{4,3,1,2,0:T(8,128)(2,1)S(1)} %copy.20), channel_id=1, replica_groups=mesh['grp'=2,'ep_0'=16,'ep_1'=2,'tp'=8] {'ep_0'}, dimensions={0} | all-to-all | bytes 786432 | tf_op jit(solution)/shard_map/all_to_all | solution.py:42
  93.2 0.1 reduce-scatter.2.cloned.1.call-start
  93.3 59.5 %all-gather.2.cloned.1.call-done = bf16[768,2048]{1,0:T(8,128)(2,1)} async-done(((bf16[768,256]{1,0:T(8,128)(2,1)}), bf16[768,2048]{1,0:T(8,128)(2,1)}) %all-gather.2.cloned.1.call-update) | async-done | bytes 3145744 | tf_op jit(solution)/shard_map/all_gather | solution.py:82
  152.8 3.8 %fusion.3 = f32[768,384]{1,0:T(8,128)S(1)} fusion(bf16[768,2048]{1,0:T(8,128)(2,1)} %all-gather.2.cloned.1.call-done, bf16[1,2048,384]{2,1,0:T(8,128)(2,1)S(1)} %copy-done.3), kind=kOutput, calls=%fused_computation.7 | convolution fusion | flops 1207959552 | bytes 5898240 | tf_op jit(solution)/shard_map/dot_general | solution.py:85
  156.6 1.8 fusion.8
  158.5 3.5 %convolution_convert_fusion = bf16[32,24,2048]{2,1,0:T(8,128)(2,1)} fusion(bf16[32,24,384]{2,1,0:T(8,128)(2,1)S(1)} %bitcast.48, bf16[1,384,2048]{2,1,0:T(8,128)(2,1)S(1)} %copy-done), kind=kOutput, calls=%fused_computation.3 | convolution fusion | flops 1209532416 | bytes 5308416 | tf_op jit(solution)/shard_map/dot_general | solution.py:88
  162.0 54.2 %reduce-scatter.2.cloned.1.call-done = bf16[32,24,256]{2,1,0:T(8,128)(2,1)} async-done(((bf16[32,24,2048]{2,1,0:T(8,128)(2,1)}), bf16[32,24,256]{2,1,0:T(8,128)(2,1)}) %reduce-scatter.2.cloned.1.call-update) | async-done | bytes 393232 | tf_op jit(solution)/shard_map/reduce_scatter | solution.py:90
  216.2 16.9 %all-to-all-start.3 = ((bf16[32,24,256]{2,1,0:T(8,128)(2,1)}), bf16[32,24,256]{2,1,0:T(8,128)(2,1)S(1)}, u32[]{:S(2)}, u32[]{:S(2)}) async-start(bf16[32,24,256]{2,1,0:T(8,128)(2,1)} %reduce-scatter.2.cloned.1.call-done), calls=%async_computation.4 | async-start | bytes 786432 | tf_op jit(solution)/shard_map/all_to_all | solution.py:93
  233.2 0.1 copy.21
  233.3 27.4 %all-to-all-done.3 = bf16[32,24,256]{2,1,0:T(8,128)(2,1)S(1)} async-done(((bf16[32,24,256]{2,1,0:T(8,128)(2,1)}), bf16[32,24,256]{2,1,0:T(8,128)(2,1)S(1)}, u32[]{:S(2)}, u32[]{:S(2)}) %all-to-all-start.3) | async-done | bytes 393248 | tf_op jit(solution)/shard_map/all_to_all | solution.py:93
  260.7 1.9 gather_fusion.1
  262.7 0.3 reshape.98
  262.9 1.4 multiply_reduce_fusion
  (27 shorter events, 0.3 us)
Async XLA Ops:
  6.5 152.0 %copy-start = (bf16[1,384,2048]{2,1,0:T(8,128)(2,1)S(1)}, bf16[1,384,2048]{2,1,0:T(8,128)(2,1)}, u32[]{:S(2)}) copy-start(bf16[1,384,2048]{2,1,0:T(8,128)(2,1)} %param.13) | copy-start | bytes 4718596
  8.3 15.0 %all-to-all-start = ((f32[8,256,1]{1,2,0:T(1,128)}), f32[8,256,1]{1,2,0:T(1,128)S(1)}, u32[]{:S(2)}, u32[]{:S(2)}) async-start(f32[8,256,1]{1,2,0:T(1,128)} %broadcast_in_dim.29), calls=%async_computation | async-start | bytes 16384 | tf_op jit(solution)/shard_map/all_to_all | solution.py:16
  16.2 136.6 %all-gather.2.cloned.1.call-start = ((), (), s32[]{:S(2)}) async-start(), calls=%async_computation.5 | async-start | bytes 3538944 | tf_op jit(solution)/shard_map/all_gather | solution.py:82
  27.1 125.6 %copy-start.3 = (bf16[1,2048,384]{2,1,0:T(8,128)(2,1)S(1)}, bf16[1,2048,384]{2,1,0:T(8,128)(2,1)}, u32[]{:S(2)}) copy-start(bf16[1,2048,384]{2,1,0:T(8,128)(2,1)} %param.11) | copy-start | bytes 4718596
  93.2 123.0 %reduce-scatter.2.cloned.1.call-start = ((), (), s32[]{:S(2)}) async-start(), calls=%async_computation.6 | async-start | bytes 3538944 | tf_op jit(solution)/shard_map/reduce_scatter | solution.py:90
  152.8 3.8 %copy-start.2 = (bf16[768,2048]{1,0:T(8,128)(2,1)S(1)}, bf16[768,2048]{1,0:T(8,128)(2,1)}, u32[]{:S(2)}) copy-start(bf16[768,2048]{1,0:T(8,128)(2,1)} %all-gather.2.cloned.1.call-done) | copy-start | bytes 9437188
  152.8 3.8 %copy-start.4 = (bf16[1,2048,384]{2,1,0:T(8,128)(2,1)S(1)}, bf16[1,2048,384]{2,1,0:T(8,128)(2,1)}, u32[]{:S(2)}) copy-start(bf16[1,2048,384]{2,1,0:T(8,128)(2,1)} %param.12) | copy-start | bytes 4718596
  162.0 71.2 %copy-start.1 = (f32[256,2]{0,1:T(2,128)S(1)}, f32[256,2]{0,1:T(2,128)}, u32[]{:S(2)}) copy-start(f32[256,2]{0,1:T(2,128)} %param.10) | copy-start | bytes 6148
  216.2 44.5 %all-to-all-start.3 = ((bf16[32,24,256]{2,1,0:T(8,128)(2,1)}), bf16[32,24,256]{2,1,0:T(8,128)(2,1)S(1)}, u32[]{:S(2)}, u32[]{:S(2)}) async-start(bf16[32,24,256]{2,1,0:T(8,128)(2,1)} %reduce-scatter.2.cloned.1.call-done), calls=%async_computation.4 | async-start | bytes 786432 | tf_op jit(solution)/shard_map/all_to_all | solution.py:93
Sparse Core Ops, SparseCore 0:
  93.3 59.4 all-gather.1
  162.2 54.0 reduce-scatter.1
where the time goes:
time: 272 us; the launch traced here: 271 us
  waiting for transfers between devices  141 us (52%)
  blocking collectives  65.9 us (24%)
  starting transfers between devices  24.9 us (9%)
  between operations  13.6 us (5%)
  local copies, waits for them, and re-layouts  10.6 us (4%)
  matrix products  9.14 us (3%)
  other arithmetic  5.77 us (2%)
    all_to_all x2, blocking collectives, moved_by_axis(): whole = lax.all_to_all(whole, axes[k], k, k, tiled=True)  65.9 us
    all_gather x1, waiting for transfers between devices, on_device(): col_piece = lax.all_gather(tok_rows, 'tp', axis=1, tiled=True)  59.5 us
    reduce_scatter x1, waiting for transfers between devices, on_device(): lax.psum_scatter(partial_value.astype(jnp.bfloat16), 'tp', scatter_dimens...  54.2 us
    all_to_all x1, waiting for transfers between devices, on_device(): lax.all_to_all(summed, EP, split_axis=0, concat_axis=0, tiled=True)  27.4 us
    all_to_all x1, starting transfers between devices, on_device(): lax.all_to_all(summed, EP, split_axis=0, concat_axis=0, tiled=True)  16.9 us
    all_to_all x1, starting transfers between devices, sent_to_all(): lax.all_to_all(jnp.broadcast_to(array[None], (count, *array.shape)), axis...  7.86 us
  transfers between devices with their start and end apart: 4, of which 3 were waited for; matrix products, arithmetic and copies ran while one was open for 3% of the time, Pallas kernels for 0%

commit v1 on v0

v1 whole, which is shorter than its diff:
```python
import functools

import jax
import jax.numpy as jnp
from jax import lax
from jax.experimental import pallas as pl
from jax.experimental.pallas import tpu as pltpu
from jax.sharding import PartitionSpec as P

MESH = pl.DeviceIdType.MESH
F32 = jnp.float32
BF16 = jnp.bfloat16
EPS = 1e-06
SLOTS = 4


def dot_nn(a, b):
    return jnp.dot(a, b, preferred_element_type=F32)


def dot_nt(a, b):
    return lax.dot_general(a, b, (((1,), (1,)), ((), ())), preferred_element_type=F32)


def stacked(y):
    rows = y.shape[0]
    left = y[:, :128].reshape(rows // 8, 1, 8, 128)
    right = y[:, 128:].reshape(rows // 8, 1, 8, 128)
    return jnp.concatenate([left, right], axis=1).reshape(2 * rows, 128)


def kernel(
    n_ep, n_tp, cap,
    tok_ref, gain_ref, ids_ref, gw_ref, wg_ref, wu_ref, wd_ref,
    out_ref,
    wgu, wdn, sbuf, xg, lhs, part, stage, rs, yout, back, wt,
    w_sem, z_send, z_recv, ag_send, ag_recv, rs_send, rs_recv, ret_send, ret_recv,
):
    n_z = n_ep // 2
    hops = n_tp // 2
    chunks = n_ep // SLOTS
    tok_count, feats = tok_ref.shape
    ff = wg_ref.shape[1]
    width = feats * n_tp
    rows = SLOTS * cap
    rows2 = 2 * rows
    half = SLOTS // 2
    me = lax.axis_index("ep")
    mt = lax.axis_index("tp")
    z, core = me // 2, me % 2
    SGN = (1, -1)

    loads = [
        pltpu.make_async_copy(wg_ref, wgu.at[:, pl.ds(0, ff)], w_sem.at[0]),
        pltpu.make_async_copy(wu_ref, wgu.at[:, pl.ds(ff, ff)], w_sem.at[1]),
        pltpu.make_async_copy(wd_ref, wdn, w_sem.at[2]),
    ]
    for load in loads:
        load.start()

    barrier = pltpu.get_barrier_semaphore()

    @pl.loop(1, n_ep)
    def _(d):
        pl.semaphore_signal(
            barrier, inc=1, device_id={"ep": (me + d) % n_ep}, device_id_type=MESH
        )

    for sg in SGN:
        pl.semaphore_signal(
            barrier, inc=1, device_id={"tp": (mt + sg + n_tp) % n_tp}, device_id_type=MESH
        )

    e_iota = lax.broadcasted_iota(jnp.int32, (n_ep, tok_count), 0)
    m0 = ids_ref[0:1, :] == e_iota
    m1 = ids_ref[1:2, :] == e_iota
    member = jnp.where(m0 | m1, 1.0, 0.0).astype(F32)
    member_b = member.astype(BF16)
    t_row = lax.broadcasted_iota(jnp.int32, (tok_count, tok_count), 0)
    t_col = lax.broadcasted_iota(jnp.int32, (tok_count, tok_count), 1)
    upper = jnp.where(t_row < t_col, 1.0, 0.0).astype(BF16)
    rank = dot_nn(member_b, upper)
    rank = jnp.where(member > 0.5, rank, -1.0).astype(BF16)
    expand = (
        lax.broadcasted_iota(jnp.int32, (n_ep, cap, n_ep), 0)
        == lax.broadcasted_iota(jnp.int32, (n_ep, cap, n_ep), 2)
    )
    expand = jnp.where(expand, 1.0, 0.0).astype(F32).reshape(n_ep * cap, n_ep).astype(BF16)
    c_iota = lax.broadcasted_iota(jnp.int32, (n_ep, cap, tok_count), 1).astype(F32)
    c_iota = c_iota.reshape(n_ep * cap, tok_count)
    pick = jnp.where(dot_nn(expand, rank) == c_iota, 1.0, 0.0).astype(BF16)
    sent = stacked(dot_nn(pick, tok_ref[...])).astype(BF16)
    sbuf[...] = sent.reshape(n_ep, 2 * cap, 128)
    xg[mt, 0] = sbuf[me]

    def offset(i):
        if n_z >= 8:
            near, tail = 3, 4
            i = i + tail * ((i + n_z - near) // n_z) - (n_z - near) * ((i + tail) // n_z)
        return ((i + 1) // 2) * (2 * (i % 2) - 1)

    def peer(j, sign):
        zz = (z + sign * offset(j // 2) + n_z) % n_z
        return zz * 2 + (core + j % 2) % 2

    def z_copy(j):
        to = peer(j, -1)
        return pltpu.make_async_remote_copy(
            src_ref=sbuf.at[to], dst_ref=xg.at[mt, j],
            send_sem=z_send.at[j], recv_sem=z_recv.at[j],
            device_id={"ep": to}, device_id_type=MESH,
        )

    def ret_copy(j):
        to = peer(j, 1)
        return pltpu.make_async_remote_copy(
            src_ref=yout.at[j], dst_ref=back.at[me],
            send_sem=ret_send.at[j], recv_sem=ret_recv.at[me],
            device_id={"ep": to}, device_id_type=MESH,
        )

    def ret_wait(e):
        pltpu.make_async_remote_copy(
            src_ref=yout.at[0], dst_ref=back.at[e],
            send_sem=ret_send.at[0], recv_sem=ret_recv.at[e],
            device_id={"ep": me}, device_id_type=MESH,
        ).wait_recv()

    def ag_copy(d, s, c, block):
        start = c * SLOTS
        count = SLOTS
        if s == hops - 1:
            start = start + (0 if d == 0 else half)
            count = half
        ref = xg.at[block, pl.ds(start, count)]
        return pltpu.make_async_remote_copy(
            src_ref=ref, dst_ref=ref,
            send_sem=ag_send.at[d, s, c], recv_sem=ag_recv.at[d, s, c],
            device_id={"tp": (mt + SGN[d] + n_tp) % n_tp}, device_id_type=MESH,
        )

    def ag_start(d, s, c):
        ag_copy(d, s, c, (mt - SGN[d] * s + n_tp) % n_tp).start()

    def ag_wait(d, s, c):
        ag_copy(d, s, c, (mt - SGN[d] * (s + 1) + n_tp) % n_tp).wait_recv()

    def rs_copy(d, r, c):
        if r == 0:
            span = pl.ds(0 if d == 0 else rows, rows)
            src, dst = stage.at[d, r, c, span], rs.at[d, r, c, span]
        else:
            src, dst = stage.at[d, r, c], rs.at[d, r, c]
        return pltpu.make_async_remote_copy(
            src_ref=src, dst_ref=dst,
            send_sem=rs_send.at[d, r, c], recv_sem=rs_recv.at[d, r, c],
            device_id={"tp": (mt + SGN[d] + n_tp) % n_tp}, device_id_type=MESH,
        )

    pl.semaphore_wait(barrier, n_ep - 1 + 2)

    @pl.loop(1, n_ep)
    def _(j):
        z_copy(j).start()

    eye = jnp.where(t_row == t_col, 1.0, 0.0).astype(BF16)
    lower = jnp.where(t_col < t_row, 1.0, 0.0).astype(BF16)
    gate_w = jnp.where(m0, gw_ref[0:1, :], 0.0) + jnp.where(m1, gw_ref[1:2, :], 0.0)
    gate_hi = gate_w.astype(BF16)
    gate_lo = (gate_w - gate_hi.astype(F32)).astype(BF16)
    rank_t = jnp.where(dot_nt(eye, member_b) > 0.5, dot_nt(lower, member_b), -1.0).astype(BF16)
    l_e = lax.broadcasted_iota(jnp.int32, (n_ep, n_ep * cap), 0) * cap
    l_s = lax.broadcasted_iota(jnp.int32, (n_ep, n_ep * cap), 1)
    expand_t = jnp.where((l_s >= l_e) & (l_s < l_e + cap), 1.0, 0.0).astype(BF16)
    lane = lax.broadcasted_iota(jnp.int32, (tok_count, n_ep * cap), 1).astype(F32)
    lane_c = lane - cap * jnp.floor((lane + 0.5) * (1.0 / cap))
    hit = dot_nn(rank_t, expand_t) == lane_c
    wt[0] = jnp.where(
        hit, dot_nn(dot_nt(eye, gate_hi).astype(BF16), expand_t), 0.0
    ).astype(BF16)
    wt[1] = jnp.where(
        hit, dot_nn(dot_nt(eye, gate_lo).astype(BF16), expand_t), 0.0
    ).astype(BF16)

    for load in loads:
        load.wait()

    def compute(c):
        total = jnp.zeros((rows // 8, 8, 128), F32)
        for b in range(n_tp):
            v = xg[b, pl.ds(c * SLOTS, SLOTS)].reshape(rows2, 128).astype(F32)
            v = v.reshape(rows // 8, 2, 8, 128)
            for h in range(2):
                vh = v[:, h]
                total = total + vh * vh
                k = 2 * b + h
                scaled = vh * gain_ref[k : k + 1, :].reshape(1, 1, 128)
                lhs[:, k * 128 : (k + 1) * 128] = scaled.reshape(rows, 128).astype(BF16)
        square = jnp.sum(total.reshape(rows, 128), axis=1, keepdims=True)
        scale = lax.rsqrt(square / width + EPS)
        gu = dot_nn(lhs[...], wgu[...])
        gate = gu[:, :ff] * scale
        up = gu[:, ff:] * scale
        hidden = (gate / (1.0 + jnp.exp(-gate)) * up).astype(BF16)
        y = dot_nn(hidden, wdn[...])
        for b in range(n_tp):
            part[c, b] = stacked(y[:, b * feats : (b + 1) * feats])

    def in_range(c):
        return (c >= 0) & (c < chunks)

    @pl.loop(0, chunks + 2 * hops)
    def _(t):
        for s in range(hops - 1, 0, -1):

            @pl.when(in_range(t - s))
            def _():
                c = t - s
                for d in range(2):
                    ag_wait(d, s - 1, c)
                    ag_start(d, s, c)

        @pl.when(t < chunks)
        def _():
            for k in range(SLOTS):
                j = t * SLOTS + k

                def arrived():
                    pltpu.make_async_remote_copy(
                        src_ref=sbuf.at[0], dst_ref=xg.at[mt, j],
                        send_sem=z_send.at[j], recv_sem=z_recv.at[j],
                        device_id={"ep": me}, device_id_type=MESH,
                    ).wait_recv()

                if k == 0:
                    pl.when(t > 0)(arrived)
                else:
                    arrived()
            for d in range(2):
                ag_start(d, 0, t)

        @pl.when(in_range(t - hops))
        def _():
            c = t - hops
            for d in range(2):
                ag_wait(d, hops - 1, c)
            compute(c)

        for r in range(hops - 1, -1, -1):

            @pl.when(in_range(t - hops - r))
            def _():
                c = t - hops - r
                for d in range(2):
                    block = (mt + SGN[d] * (hops - r) + n_tp) % n_tp
                    own = slice(0, rows) if d == 0 else slice(rows, rows2)
                    rest = slice(rows, rows2) if d == 0 else slice(0, rows)
                    if r == 0:
                        stage[d, r, c, own] = part[c, block, own].astype(BF16)
                    elif r == 1:
                        rs_copy(d, 0, c).wait_recv()
                        stage[d, r, c, own] = (
                            part[c, block, own] + rs[d, 0, c, own].astype(F32)
                        ).astype(BF16)
                        stage[d, r, c, rest] = part[c, block, rest].astype(BF16)
                    else:
                        rs_copy(d, r - 1, c).wait_recv()
                        stage[d, r, c] = (
                            part[c, block] + rs[d, r - 1, c].astype(F32)
                        ).astype(BF16)
                    rs_copy(d, r, c).start()

        @pl.when(in_range(t - 2 * hops))
        def _():
            c = t - 2 * hops
            for d in range(2):
                rs_copy(d, hops - 1, c).wait_recv()
            y = (
                part[c, mt]
                + rs[0, hops - 1, c].astype(F32)
                + rs[1, hops - 1, c].astype(F32)
            ).astype(BF16)
            yout[pl.ds(c * SLOTS, SLOTS)] = y.reshape(SLOTS, 2 * cap, 128)
            for k in range(SLOTS):
                j = c * SLOTS + k
                if k == 0:

                    @pl.when(c > 0)
                    def _():
                        ret_copy(j).start()
                else:
                    ret_copy(j).start()

    back[me] = yout[0]

    @pl.loop(1, n_ep)
    def _(d):
        ret_wait((me + d) % n_ep)

    b4 = back[...].reshape(2 * n_ep * cap, 128).astype(F32)
    b4 = b4.reshape(n_ep * cap // 8, 2, 8, 128)
    left = b4[:, 0].reshape(n_ep * cap, 128).astype(BF16)
    right = b4[:, 1].reshape(n_ep * cap, 128).astype(BF16)
    picked = jnp.concatenate([left, right], axis=1)
    out_ref[...] = (dot_nn(wt[0], picked) + dot_nn(wt[1], picked)).astype(BF16)

    @pl.loop(1, n_ep)
    def _(j):
        z_copy(j).wait_send()
        ret_copy(j).wait_send()

    @pl.loop(0, chunks)
    def _(c):
        for d in range(2):
            for s in range(hops):
                ag_copy(d, s, c, mt).wait_send()
                rs_copy(d, s, c).wait_send()


def on_device(n_ep, n_tp, tokens, norm_gain, expert_ids, gate_weights, w_gate, w_up, w_down):
    tok_count, feats = tokens.shape
    cap = 3 * tok_count * expert_ids.shape[1] // (2 * n_ep)
    width, ff = w_gate.shape[1:]
    chunks, hops = n_ep // SLOTS, n_tp // 2
    rows = SLOTS * cap
    vmem = pl.BlockSpec(memory_space=pltpu.VMEM)
    hbm = pl.BlockSpec(memory_space=pl.ANY)
    dma = pltpu.SemaphoreType.DMA
    block = (n_ep, 2 * cap, 128)
    return pl.pallas_call(
        functools.partial(kernel, n_ep, n_tp, cap),
        out_shape=jax.ShapeDtypeStruct((tok_count, feats), BF16),
        in_specs=[vmem, vmem, vmem, vmem, hbm, hbm, hbm],
        out_specs=vmem,
        scratch_shapes=[
            pltpu.VMEM((width, 2 * ff), BF16),
            pltpu.VMEM((ff, width), BF16),
            pltpu.VMEM(block, BF16),
            pltpu.VMEM((n_tp, *block), BF16),
            pltpu.VMEM((rows, width), BF16),
            pltpu.VMEM((chunks, n_tp, 2 * rows, 128), F32),
            pltpu.VMEM((2, hops, chunks, 2 * rows, 128), BF16),
            pltpu.VMEM((2, hops, chunks, 2 * rows, 128), BF16),
            pltpu.VMEM(block, BF16),
            pltpu.VMEM(block, BF16),
            pltpu.VMEM((2, tok_count, n_ep * cap), BF16),
            dma((3,)),
            dma((n_ep,)),
            dma((n_ep,)),
            dma((2, hops, chunks)),
            dma((2, hops, chunks)),
            dma((2, hops, chunks)),
            dma((2, hops, chunks)),
            dma((n_ep,)),
            dma((n_ep,)),
        ],
        compiler_params=pltpu.CompilerParams(
            collective_id=0, has_side_effects=True, vmem_limit_bytes=48 * 1024 * 1024
        ),
    )(
        tokens,
        norm_gain.reshape(-1, 128),
        expert_ids.T,
        gate_weights.T,
        w_gate[0],
        w_up[0],
        w_down[0],
    )


def solution(mesh):
    rows = ("grp", "ep")
    return jax.shard_map(
        functools.partial(on_device, mesh.shape["ep"], mesh.shape["tp"]),
        mesh=mesh,
        in_specs=(
            P(rows, "tp"),
            P(),
            P(rows, None),
            P(rows, None),
            P("ep", None, "tp"),
            P("ep", None, "tp"),
            P("ep", "tp", None),
        ),
        out_specs=P(rows, "tp"),
        check_vma=False,
    )
```

time: 272 us -> 144 us (0.53)
  waiting for transfers between devices: 141 us -> 0 us
  Pallas kernels: 0 us -> 135 us
  blocking collectives: 65.9 us -> 0 us
  starting transfers between devices: 24.9 us -> 0 us
  between operations: 13.6 us -> 0.02 us
  matrix products: 9.14 us -> 0 us
  other arithmetic: 5.77 us -> 0 us
  local copies, waits for them, and re-layouts: 10.6 us -> 7.84 us
    pallas_call x0 -> x1, Pallas kernels: none -> 135 us  [on_device(): pl.pallas_call(functools.partial(kernel, n_ep, n_tp, cap), out_shape=jax....]
    all_to_all x2 -> x0, blocking collectives: 65.9 us -> none  [moved_by_axis(): whole = lax.all_to_all(whole, axes[k], k, k, tiled=True)]
    all_gather x1 -> x0, waiting for transfers between devices: 59.5 us -> none  [on_device(): col_piece = lax.all_gather(tok_rows, 'tp', axis=1, tiled=True)]
    reduce_scatter x1 -> x0, waiting for transfers between devices: 54.2 us -> none  [on_device(): lax.psum_scatter(partial_value.astype(jnp.bfloat16), 'tp', scatter_dimens...]
    all_to_all x2 -> x0, waiting for transfers between devices: 27.4 us -> none  [the longest x1 27.4 us: on_device(): lax.all_to_all(summed, EP, split_axis=0, concat_axis=0, tiled=True)]
    all_to_all x2 -> x0, starting transfers between devices: 24.8 us -> none  [the longest x1 16.9 us: on_device(): lax.all_to_all(summed, EP, split_axis=0, concat_axis=0, tiled=True)]
    dot_general x3 -> x0, matrix products: 9.14 us -> none  [the longest x1 3.83 us: on_device(): jnp.dot(col_piece, gate_rows, preferred_element_type=jnp.float32)]
    unnamed x12 -> x15, local copies, waits for them, and re-layouts: 0.97 us -> 7.84 us
  transfers between devices with their start and end apart: 4 -> 0, of which waited for: 3 -> 0; matrix products, arithmetic and copies ran while one was open for 3% -> 0% of each run, Pallas kernels for 0% -> 0%
where the time goes in v1:
time: 144 us; the launch traced here: 143 us
  Pallas kernels  135 us (94%)
  local copies, waits for them, and re-layouts  7.84 us (5%)
    pallas_call x1, Pallas kernels, on_device(): pl.pallas_call(functools.partial(kernel, n_ep, n_tp, cap), out_shape=jax....  135 us
    unnamed x15, local copies, waits for them, and re-layouts  7.84 us

profile of v1, /device:TPU:65, one launch (start us, length us, event | category | flops | bytes accessed | tf_op | source)
XLA Modules:
  0.0 143.2 jit_solution(7878946248468808133)
XLA Ops:
  0.0 0.0 copy-start
  0.0 1.4 copy-done
  1.4 0.0 copy-start.1
  1.4 1.4 copy-done.1
  2.8 0.0 copy-start.2
  2.8 1.4 copy-done.2
  4.2 0.0 copy-start.3
  4.2 0.9 copy-done.3
  5.1 0.0 copy-start.4
  5.1 0.7 copy-done.4
  5.8 0.0 copy-start.5
  5.8 0.7 copy-done.5
  6.5 0.0 copy-start.6
  6.5 0.7 copy-done.6
  7.2 135.3 %shard_map.73 = bf16[256,256]{1,0:T(8,128)(2,1)S(1)} custom-call(bf16[256,256]{1,0:T(8,128)(2,1)S(1)} %copy-done.3, f32[16,128]{1,0:T(8,128)S(1)} %bitcast.9, s32[2,256]{1,0:T(2,128)S(1)} %bitcast.10, f32[2,256]{1,0:T(2,128)S(1)} %bitcast.11, bf16[2048,384]{1,0:T(8,128)(2,1)S(1)} %bitcast.6, bf16[2048,384]{1,0:T(8,128)(2,1)S(1)} %bitcast.7, ...), custom_call_target="tpu_custom_call" | custom-call | tf_op jit(solution)/shard_map/pallas_call | solution.py:330
  142.5 0.7 copy.9
Async XLA Ops:
  0.0 1.4 copy-start
  1.4 1.4 copy-start.1
  2.8 1.4 copy-start.2
  4.2 0.9 copy-start.3
  5.1 0.7 copy-start.4
  5.8 0.7 copy-start.5
  6.5 0.7 copy-start.6

commit v2 on v1

v2 whole, which is shorter than its diff:
```python
import functools

import jax
import jax.numpy as jnp
from jax import lax
from jax.experimental import pallas as pl
from jax.experimental.pallas import tpu as pltpu
from jax.sharding import PartitionSpec as P

MESH = pl.DeviceIdType.MESH
F32 = jnp.float32
BF16 = jnp.bfloat16
EPS = 1e-06
SLOTS = 4
GROUP = 2
STEPS = (0, 1, 4, -4, 5, -5, 6, -6, 7, -7, 8, 3, -3, 2, -2, -1)


def steps_of(n_z):
    if n_z == len(STEPS):
        return list(STEPS)
    return [0] + [(i + 1) // 2 * (1 if i % 2 else -1) for i in range(1, n_z)]


def dot_nn(a, b):
    return jnp.dot(a, b, preferred_element_type=F32)


def dot_nt(a, b):
    return lax.dot_general(a, b, (((1,), (1,)), ((), ())), preferred_element_type=F32)


def stacked(y):
    rows = y.shape[0]
    left = y[:, :128].reshape(rows // 8, 1, 8, 128)
    right = y[:, 128:].reshape(rows // 8, 1, 8, 128)
    return jnp.concatenate([left, right], axis=1).reshape(2 * rows, 128)


def kernel(
    n_ep, n_tp, cap,
    tok_hbm, gain_hbm, ids_hbm, gw_hbm, wg_ref, wu_ref, wd_ref,
    out_ref,
    tok_ref, gain_ref, ids_ref, gw_ref,
    wgu, wdn, sbuf, xg, lhs, part, stage, rs, yout, back, wt,
    in_sem, w_sem, z_send, z_recv, ag_send, ag_recv, rs_send, rs_recv, ret_send, ret_recv,
):
    n_z = n_ep // 2
    hops = n_tp // 2
    chunks = n_ep // SLOTS
    groups = chunks // GROUP
    wide = GROUP * SLOTS
    tok_count, feats = tok_ref.shape
    ff = wg_ref.shape[1]
    width = feats * n_tp
    rows = SLOTS * cap
    rows2 = 2 * rows
    grows = wide * cap
    half = SLOTS // 2
    me = lax.axis_index("ep")
    mt = lax.axis_index("tp")
    z, core = me // 2, me % 2
    SGN = (1, -1)

    ins = [
        pltpu.make_async_copy(ids_hbm, ids_ref, in_sem.at[0]),
        pltpu.make_async_copy(tok_hbm, tok_ref, in_sem.at[1]),
        pltpu.make_async_copy(gw_hbm, gw_ref, in_sem.at[2]),
        pltpu.make_async_copy(gain_hbm, gain_ref, in_sem.at[3]),
    ]
    for load in ins:
        load.start()

    barrier = pltpu.get_barrier_semaphore()

    @pl.loop(1, n_ep)
    def _(d):
        pl.semaphore_signal(
            barrier, inc=1, device_id={"ep": (me + d) % n_ep}, device_id_type=MESH
        )

    for sg in SGN:
        pl.semaphore_signal(
            barrier, inc=1, device_id={"tp": (mt + sg + n_tp) % n_tp}, device_id_type=MESH
        )

    loads = [
        pltpu.make_async_copy(wg_ref, wgu.at[:, pl.ds(0, ff)], w_sem.at[0]),
        pltpu.make_async_copy(wu_ref, wgu.at[:, pl.ds(ff, ff)], w_sem.at[1]),
        pltpu.make_async_copy(wd_ref, wdn, w_sem.at[2]),
    ]
    for load in loads:
        load.start()

    steps = steps_of(n_z)

    def peer(j, sign):
        zz = (z + sign * steps[j // 2] + n_z) % n_z
        return zz * 2 + (core + j % 2) % 2

    for load in ins:
        load.wait()
    j_iota = lax.broadcasted_iota(jnp.int32, (n_ep, 1), 0)
    e_iota = jnp.zeros((n_ep, 1), jnp.int32)
    for j in range(n_ep):
        e_iota = jnp.where(j_iota == j, peer(j, -1), e_iota)
    m0 = ids_ref[0:1, :] == e_iota
    m1 = ids_ref[1:2, :] == e_iota
    member = jnp.where(m0 | m1, 1.0, 0.0).astype(F32)
    member_b = member.astype(BF16)
    t_row = lax.broadcasted_iota(jnp.int32, (tok_count, tok_count), 0)
    t_col = lax.broadcasted_iota(jnp.int32, (tok_count, tok_count), 1)
    upper = jnp.where(t_row < t_col, 1.0, 0.0).astype(BF16)
    rank = dot_nn(member_b, upper)
    rank = jnp.where(member > 0.5, rank, -1.0).astype(BF16)
    x_row = lax.broadcasted_iota(jnp.int32, (wide, cap, n_ep), 0)
    x_col = lax.broadcasted_iota(jnp.int32, (wide, cap, n_ep), 2)
    c_iota = lax.broadcasted_iota(jnp.int32, (wide, cap, tok_count), 1).astype(F32)
    c_iota = c_iota.reshape(grows, tok_count)

    def z_copy(j):
        return pltpu.make_async_remote_copy(
            src_ref=sbuf.at[j], dst_ref=xg.at[mt, j],
            send_sem=z_send.at[j], recv_sem=z_recv.at[j],
            device_id={"ep": peer(j, -1)}, device_id_type=MESH,
        )

    def ret_copy(j):
        return pltpu.make_async_remote_copy(
            src_ref=yout.at[j], dst_ref=back.at[j],
            send_sem=ret_send.at[j], recv_sem=ret_recv.at[j],
            device_id={"ep": peer(j, 1)}, device_id_type=MESH,
        )

    for g in range(groups):
        expand = jnp.where(x_row + g * wide == x_col, 1.0, 0.0).astype(F32)
        expand = expand.reshape(grows, n_ep).astype(BF16)
        pick = jnp.where(dot_nn(expand, rank) == c_iota, 1.0, 0.0).astype(BF16)
        sent = stacked(dot_nn(pick, tok_ref[...])).astype(BF16)
        sbuf[g * wide : (g + 1) * wide] = sent.reshape(wide, 2 * cap, 128)
        if g == 0:
            xg[mt, 0] = sbuf[0]
            pl.semaphore_wait(barrier, n_ep - 1 + 2)

        for j in range(max(1, g * wide), (g + 1) * wide):
            z_copy(j).start()

    def ag_copy(d, s, c, block):
        start = c * SLOTS
        count = SLOTS
        if s == hops - 1:
            start = start + (0 if d == 0 else half)
            count = half
        ref = xg.at[block, pl.ds(start, count)]
        return pltpu.make_async_remote_copy(
            src_ref=ref, dst_ref=ref,
            send_sem=ag_send.at[d, s, c], recv_sem=ag_recv.at[d, s, c],
            device_id={"tp": (mt + SGN[d] + n_tp) % n_tp}, device_id_type=MESH,
        )

    def ag_start(d, s, c):
        ag_copy(d, s, c, (mt - SGN[d] * s + n_tp) % n_tp).start()

    def ag_wait(d, s, c):
        ag_copy(d, s, c, (mt - SGN[d] * (s + 1) + n_tp) % n_tp).wait_recv()

    def rs_copy(d, r, c):
        if r == 0:
            span = pl.ds(0 if d == 0 else rows, rows)
            src, dst = stage.at[d, r, c, span], rs.at[d, r, c, span]
        else:
            src, dst = stage.at[d, r, c], rs.at[d, r, c]
        return pltpu.make_async_remote_copy(
            src_ref=src, dst_ref=dst,
            send_sem=rs_send.at[d, r, c], recv_sem=rs_recv.at[d, r, c],
            device_id={"tp": (mt + SGN[d] + n_tp) % n_tp}, device_id_type=MESH,
        )

    def combine_weights():
        eye = jnp.where(t_row == t_col, 1.0, 0.0).astype(BF16)
        lower = jnp.where(t_col < t_row, 1.0, 0.0).astype(BF16)
        gate_w = jnp.where(m0, gw_ref[0:1, :], 0.0) + jnp.where(m1, gw_ref[1:2, :], 0.0)
        gate_hi = gate_w.astype(BF16)
        gate_lo = (gate_w - gate_hi.astype(F32)).astype(BF16)
        rank_t = jnp.where(dot_nt(eye, member_b) > 0.5, dot_nt(lower, member_b), -1.0)
        rank_t = rank_t.astype(BF16)
        hi_t = dot_nt(eye, gate_hi).astype(BF16)
        lo_t = dot_nt(eye, gate_lo).astype(BF16)
        l_e = lax.broadcasted_iota(jnp.int32, (n_ep, grows), 0) * cap
        l_s = lax.broadcasted_iota(jnp.int32, (n_ep, grows), 1)
        lane = lax.broadcasted_iota(jnp.int32, (tok_count, grows), 1).astype(F32)
        lane = lane - cap * jnp.floor((lane + 0.5) * (1.0 / cap))
        for g in range(groups):
            s = l_s + g * grows
            expand_t = jnp.where((s >= l_e) & (s < l_e + cap), 1.0, 0.0).astype(BF16)
            hit = dot_nn(rank_t, expand_t) == lane
            wt[g, 0] = jnp.where(hit, dot_nn(hi_t, expand_t), 0.0).astype(BF16)
            wt[g, 1] = jnp.where(hit, dot_nn(lo_t, expand_t), 0.0).astype(BF16)

    def compute(c):
        total = jnp.zeros((rows // 8, 8, 128), F32)
        for b in range(n_tp):
            v = xg[b, pl.ds(c * SLOTS, SLOTS)].reshape(rows2, 128).astype(F32)
            v = v.reshape(rows // 8, 2, 8, 128)
            for h in range(2):
                vh = v[:, h]
                total = total + vh * vh
                k = 2 * b + h
                scaled = vh * gain_ref[k : k + 1, :].reshape(1, 1, 128)
                lhs[:, k * 128 : (k + 1) * 128] = scaled.reshape(rows, 128).astype(BF16)
        square = jnp.sum(total.reshape(rows, 128), axis=1, keepdims=True)
        scale = lax.rsqrt(square / width + EPS)
        gu = dot_nn(lhs[...], wgu[...])
        gate = gu[:, :ff] * scale
        up = gu[:, ff:] * scale
        hidden = (gate / (1.0 + jnp.exp(-gate)) * up).astype(BF16)
        y = dot_nn(hidden, wdn[...])
        for b in range(n_tp):
            part[c, b] = stacked(y[:, b * feats : (b + 1) * feats])

    def reduce_step(d, r, c):
        block = (mt + SGN[d] * (hops - r) + n_tp) % n_tp
        own = slice(0, rows) if d == 0 else slice(rows, rows2)
        rest = slice(rows, rows2) if d == 0 else slice(0, rows)
        if r == 0:
            stage[d, r, c, own] = part[c, block, own].astype(BF16)
        elif r == 1:
            rs_copy(d, 0, c).wait_recv()
            stage[d, r, c, own] = (
                part[c, block, own] + rs[d, 0, c, own].astype(F32)
            ).astype(BF16)
            stage[d, r, c, rest] = part[c, block, rest].astype(BF16)
        else:
            rs_copy(d, r - 1, c).wait_recv()
            stage[d, r, c] = (part[c, block] + rs[d, r - 1, c].astype(F32)).astype(BF16)
        rs_copy(d, r, c).start()

    def z_arrived(j):
        pltpu.make_async_remote_copy(
            src_ref=sbuf.at[0], dst_ref=xg.at[mt, j],
            send_sem=z_send.at[j], recv_sem=z_recv.at[j],
            device_id={"ep": me}, device_id_type=MESH,
        ).wait_recv()

    def gather_first(c, skip):
        for k in range(skip, SLOTS):
            z_arrived(c * SLOTS + k)
        for d in range(2):
            ag_start(d, 0, c)

    def gather_next(s, c):
        for d in range(2):
            ag_wait(d, s - 1, c)
            ag_start(d, s, c)

    def finish(c):
        for d in range(2):
            rs_copy(d, hops - 1, c).wait_recv()
        y = (
            part[c, mt]
            + rs[0, hops - 1, c].astype(F32)
            + rs[1, hops - 1, c].astype(F32)
        ).astype(BF16)
        yout[pl.ds(c * SLOTS, SLOTS)] = y.reshape(SLOTS, 2 * cap, 128)
        for cc in range(chunks):

            @pl.when(c == cc)
            def _():
                for k in range(SLOTS):
                    if cc or k:
                        ret_copy(cc * SLOTS + k).start()

    def computed(t, delay, f):
        first = t - hops - delay

        @pl.when((first >= 0) & (first < chunks - 1))
        def _():
            pl.loop(first, first + 1 + (first + 1) // (chunks - 1))(f)

    @pl.loop(0, chunks - 1 + 2 * hops)
    def _(t):
        @pl.when(t == hops)
        def _():
            for load in loads:
                load.wait()

        @functools.partial(computed, t, 0)
        def _(c):
            for d in range(2):
                ag_wait(d, hops - 1, c)
            compute(c)
            for d in range(2):
                reduce_step(d, 0, c)

        for s in range(hops - 1, 0, -1):

            @pl.when(t == s)
            def _():
                gather_next(s, 0)

            @pl.when((t - s + 1 >= 1) & (t - s + 1 < chunks))
            def _():
                gather_next(s, t - s + 1)

        @pl.when(t == 0)
        def _():
            gather_first(0, 1)

        @pl.when(t + 1 < chunks)
        def _():
            gather_first(t + 1, 0)

        pl.when(t == 0)(combine_weights)

        for r in range(1, hops):

            @functools.partial(computed, t, r)
            def _(c):
                for d in range(2):
                    reduce_step(d, r, c)

        computed(t, hops, finish)

    back[0] = yout[0]
    mixed = jnp.zeros((tok_count, feats), F32)
    for g in range(groups):

        for j in range(max(1, g * wide), (g + 1) * wide):
            ret_copy(j).wait_recv()

        b4 = back[g * wide : (g + 1) * wide].reshape(2 * grows, 128).astype(F32)
        b4 = b4.reshape(grows // 8, 2, 8, 128)
        left = b4[:, 0].reshape(grows, 128).astype(BF16)
        right = b4[:, 1].reshape(grows, 128).astype(BF16)
        picked = jnp.concatenate([left, right], axis=1)
        mixed = mixed + dot_nn(wt[g, 0], picked) + dot_nn(wt[g, 1], picked)
    out_ref[...] = mixed.astype(BF16)

    for j in range(1, n_ep):
        z_copy(j).wait_send()
        ret_copy(j).wait_send()

    @pl.loop(0, chunks)
    def _(c):
        for d in range(2):
            for s in range(hops):
                ag_copy(d, s, c, mt).wait_send()
                rs_copy(d, s, c).wait_send()


def on_device(n_ep, n_tp, tokens, norm_gain, expert_ids, gate_weights, w_gate, w_up, w_down):
    tok_count, feats = tokens.shape
    cap = 3 * tok_count * expert_ids.shape[1] // (2 * n_ep)
    width, ff = w_gate.shape[1:]
    chunks, hops = n_ep // SLOTS, n_tp // 2
    rows = SLOTS * cap
    vmem = pl.BlockSpec(memory_space=pltpu.VMEM)
    hbm = pl.BlockSpec(memory_space=pl.ANY)
    dma = pltpu.SemaphoreType.DMA
    block = (n_ep, 2 * cap, 128)
    return pl.pallas_call(
        functools.partial(kernel, n_ep, n_tp, cap),
        out_shape=jax.ShapeDtypeStruct((tok_count, feats), BF16),
        in_specs=[hbm] * 7,
        out_specs=vmem,
        scratch_shapes=[
            pltpu.VMEM((tok_count, feats), BF16),
            pltpu.VMEM((width // 128, 128), F32),
            pltpu.VMEM((2, tok_count), jnp.int32),
            pltpu.VMEM((2, tok_count), F32),
            pltpu.VMEM((width, 2 * ff), BF16),
            pltpu.VMEM((ff, width), BF16),
            pltpu.VMEM(block, BF16),
            pltpu.VMEM((n_tp, *block), BF16),
            pltpu.VMEM((rows, width), BF16),
            pltpu.VMEM((chunks, n_tp, 2 * rows, 128), F32),
            pltpu.VMEM((2, hops, chunks, 2 * rows, 128), BF16),
            pltpu.VMEM((2, hops, chunks, 2 * rows, 128), BF16),
            pltpu.VMEM(block, BF16),
            pltpu.VMEM(block, BF16),
            pltpu.VMEM((chunks // GROUP, 2, tok_count, GROUP * rows), BF16),
            dma((4,)),
            dma((3,)),
            dma((n_ep,)),
            dma((n_ep,)),
            dma((2, hops, chunks)),
            dma((2, hops, chunks)),
            dma((2, hops, chunks)),
            dma((2, hops, chunks)),
            dma((n_ep,)),
            dma((n_ep,)),
        ],
        compiler_params=pltpu.CompilerParams(
            collective_id=0, has_side_effects=True
        ),
    )(
        tokens,
        norm_gain.reshape(-1, 128),
        expert_ids.T,
        gate_weights.T,
        w_gate[0],
        w_up[0],
        w_down[0],
    )


def solution(mesh):
    rows = ("grp", "ep")
    return jax.shard_map(
        functools.partial(on_device, mesh.shape["ep"], mesh.shape["tp"]),
        mesh=mesh,
        in_specs=(
            P(rows, "tp"),
            P(),
            P(rows, None),
            P(rows, None),
            P("ep", None, "tp"),
            P("ep", None, "tp"),
            P("ep", "tp", None),
        ),
        out_specs=P(rows, "tp"),
        check_vma=False,
    )
```

time: 144 us -> 133 us (0.924)
  local copies, waits for them, and re-layouts: 7.84 us -> 1.57 us
  Pallas kernels: 135 us -> 132 us
    unnamed x15 -> x1, local copies, waits for them, and re-layouts: 7.84 us -> 1.57 us
    pallas_call x1, Pallas kernels: 135 us -> 132 us  [on_device(): pl.pallas_call(functools.partial(kernel, n_ep, n_tp, cap), out_shape=jax....]
where the time goes in v2:
time: 133 us
  Pallas kernels  132 us (99%)
  local copies, waits for them, and re-layouts  1.57 us (1%)
    pallas_call x1, Pallas kernels, on_device(): pl.pallas_call(functools.partial(kernel, n_ep, n_tp, cap), out_shape=jax....  132 us

profile of v2, /device:TPU:65, one launch (start us, length us, event | category | flops | bytes accessed | tf_op | source)
XLA Modules:
  0.0 133.4 jit_solution(2398055077913372894)
XLA Ops:
  0.0 131.8 %shard_map.73 = bf16[256,256]{1,0:T(8,128)(2,1)} custom-call(bf16[256,256]{1,0:T(8,128)(2,1)} %tok_hbm.1, f32[16,128]{1,0:T(8,128)} %bitcast.9, s32[2,256]{1,0:T(2,128)} %bitcast.10, f32[2,256]{1,0:T(2,128)} %bitcast.11, bf16[2048,384]{1,0:T(8,128)(2,1)} %bitcast.6, bf16[2048,384]{1,0:T(8,128)(2,1)} %bitcast.7, bf16[384,2048]{1,0:T(8,128)(2,1)} %bitcast.8), custom_call_target="tpu_custom_call" | custom-call | tf_op jit(solution)/shard_map/pallas_call | solution.py:361
  131.8 1.6 %copy.9 = bf16[256,256]{1,0:T(8,128)(2,1)} copy(bf16[256,256]{1,0:T(8,128)(2,1)} %shard_map.73) | data formatting | bytes 262144

commit v3 on v2

--- a/solution.py
+++ b/solution.py
@@ -73,8 +73,9 @@
 
     barrier = pltpu.get_barrier_semaphore()
 
-    @pl.loop(1, n_ep)
-    def _(d):
+    @pl.loop(0, n_ep - 1)
+    def _(i):
+        d = n_ep // 2 + ((i + 1) // 2) * (1 - 2 * (i % 2))
         pl.semaphore_signal(
             barrier, inc=1, device_id={"ep": (me + d) % n_ep}, device_id_type=MESH
         )
@@ -121,14 +122,14 @@
     def z_copy(j):
         return pltpu.make_async_remote_copy(
             src_ref=sbuf.at[j], dst_ref=xg.at[mt, j],
-            send_sem=z_send.at[j], recv_sem=z_recv.at[j],
+            send_sem=z_send, recv_sem=z_recv.at[j // SLOTS],
             device_id={"ep": peer(j, -1)}, device_id_type=MESH,
         )
 
     def ret_copy(j):
         return pltpu.make_async_remote_copy(
             src_ref=yout.at[j], dst_ref=back.at[j],
-            send_sem=ret_send.at[j], recv_sem=ret_recv.at[j],
+            send_sem=ret_send, recv_sem=ret_recv.at[j // wide],
             device_id={"ep": peer(j, 1)}, device_id_type=MESH,
         )
 
@@ -154,7 +155,7 @@
         ref = xg.at[block, pl.ds(start, count)]
         return pltpu.make_async_remote_copy(
             src_ref=ref, dst_ref=ref,
-            send_sem=ag_send.at[d, s, c], recv_sem=ag_recv.at[d, s, c],
+            send_sem=ag_send, recv_sem=ag_recv.at[d, s, c],
             device_id={"tp": (mt + SGN[d] + n_tp) % n_tp}, device_id_type=MESH,
         )
 
@@ -172,7 +173,7 @@
             src, dst = stage.at[d, r, c], rs.at[d, r, c]
         return pltpu.make_async_remote_copy(
             src_ref=src, dst_ref=dst,
-            send_sem=rs_send.at[d, r, c], recv_sem=rs_recv.at[d, r, c],
+            send_sem=rs_send, recv_sem=rs_recv.at[d, r, c],
             device_id={"tp": (mt + SGN[d] + n_tp) % n_tp}, device_id_type=MESH,
         )
 
@@ -235,16 +236,15 @@
             stage[d, r, c] = (part[c, block] + rs[d, r - 1, c].astype(F32)).astype(BF16)
         rs_copy(d, r, c).start()
 
-    def z_arrived(j):
-        pltpu.make_async_remote_copy(
-            src_ref=sbuf.at[0], dst_ref=xg.at[mt, j],
-            send_sem=z_send.at[j], recv_sem=z_recv.at[j],
+    def bytes_of(ref, send_sem, recv_sem):
+        return pltpu.make_async_remote_copy(
+            src_ref=ref, dst_ref=ref, send_sem=send_sem, recv_sem=recv_sem,
             device_id={"ep": me}, device_id_type=MESH,
-        ).wait_recv()
+        )
 
     def gather_first(c, skip):
-        for k in range(skip, SLOTS):
-            z_arrived(c * SLOTS + k)
+        slots = pl.ds(c * SLOTS + skip, SLOTS - skip)
+        bytes_of(xg.at[mt, slots], z_send, z_recv.at[c]).wait_recv()
         for d in range(2):
             ag_start(d, 0, c)
 
@@ -321,12 +321,19 @@
 
         computed(t, hops, finish)
 
+    others = pl.ds(1, n_ep - 1)
+    blocks = xg.at[pl.ds(0, n_tp - 1)]
+    bytes_of(sbuf.at[others], z_send, z_recv.at[0]).wait_send()
+    bytes_of(blocks, ag_send, z_recv.at[0]).wait_send()
+    bytes_of(blocks, rs_send, z_recv.at[0]).wait_send()
+
     back[0] = yout[0]
     mixed = jnp.zeros((tok_count, feats), F32)
     for g in range(groups):
 
-        for j in range(max(1, g * wide), (g + 1) * wide):
-            ret_copy(j).wait_recv()
+        first = max(1, g * wide)
+        arrived = back.at[pl.ds(first, (g + 1) * wide - first)]
+        bytes_of(arrived, ret_send, ret_recv.at[g]).wait_recv()
 
         b4 = back[g * wide : (g + 1) * wide].reshape(2 * grows, 128).astype(F32)
         b4 = b4.reshape(grows // 8, 2, 8, 128)
@@ -336,16 +343,7 @@
         mixed = mixed + dot_nn(wt[g, 0], picked) + dot_nn(wt[g, 1], picked)
     out_ref[...] = mixed.astype(BF16)
 
-    for j in range(1, n_ep):
-        z_copy(j).wait_send()
-        ret_copy(j).wait_send()
-
-    @pl.loop(0, chunks)
-    def _(c):
-        for d in range(2):
-            for s in range(hops):
-                ag_copy(d, s, c, mt).wait_send()
-                rs_copy(d, s, c).wait_send()
+    bytes_of(yout.at[others], ret_send, ret_recv.at[0]).wait_send()
 
 
 def on_device(n_ep, n_tp, tokens, norm_gain, expert_ids, gate_weights, w_gate, w_up, w_down):
@@ -381,14 +379,14 @@
             pltpu.VMEM((chunks // GROUP, 2, tok_count, GROUP * rows), BF16),
             dma((4,)),
             dma((3,)),
-            dma((n_ep,)),
-            dma((n_ep,)),
+            dma,
+            dma((chunks,)),
+            dma,
             dma((2, hops, chunks)),
+            dma,
             dma((2, hops, chunks)),
-            dma((2, hops, chunks)),
-            dma((2, hops, chunks)),
-            dma((n_ep,)),
-            dma((n_ep,)),
+            dma,
+            dma((chunks // GROUP,)),
         ],
         compiler_params=pltpu.CompilerParams(
             collective_id=0, has_side_effects=True

time: 133 us -> 130 us (0.977)
  Pallas kernels: 132 us -> 129 us
    pallas_call x1, Pallas kernels: 132 us -> 129 us  [on_device(): pl.pallas_call(functools.partial(kernel, n_ep, n_tp, cap), out_shape=jax....]
where the time goes in v3:
time: 130 us
  Pallas kernels  129 us (99%)
  local copies, waits for them, and re-layouts  1.57 us (1%)
    pallas_call x1, Pallas kernels, on_device(): pl.pallas_call(functools.partial(kernel, n_ep, n_tp, cap), out_shape=jax....  129 us

profile of v3, /device:TPU:65, one launch (start us, length us, event | category | flops | bytes accessed | tf_op | source)
XLA Modules:
  0.0 130.1 jit_solution(5723282608353110747)
XLA Ops:
  0.0 128.5 %shard_map.73 = bf16[256,256]{1,0:T(8,128)(2,1)} custom-call(bf16[256,256]{1,0:T(8,128)(2,1)} %tok_hbm.1, f32[16,128]{1,0:T(8,128)} %bitcast.9, s32[2,256]{1,0:T(2,128)} %bitcast.10, f32[2,256]{1,0:T(2,128)} %bitcast.11, bf16[2048,384]{1,0:T(8,128)(2,1)} %bitcast.6, bf16[2048,384]{1,0:T(8,128)(2,1)} %bitcast.7, bf16[384,2048]{1,0:T(8,128)(2,1)} %bitcast.8), custom_call_target="tpu_custom_call" | custom-call | tf_op jit(solution)/shard_map/pallas_call | solution.py:359
  128.5 1.6 %copy.9 = bf16[256,256]{1,0:T(8,128)(2,1)} copy(bf16[256,256]{1,0:T(8,128)(2,1)} %shard_map.73) | data formatting | bytes 262144

commit v4 on v3

--- a/solution.py
+++ b/solution.py
@@ -13,7 +13,7 @@
 EPS = 1e-06
 SLOTS = 4
 GROUP = 2
-STEPS = (0, 1, 4, -4, 5, -5, 6, -6, 7, -7, 8, 3, -3, 2, -2, -1)
+STEPS = (0, 1, 3, -4, 5, -5, 6, -6, 8, -7, 7, 4, -3, 2, -2, -1)
 
 
 def steps_of(n_z):

time: 130 us -> 130 us (level)
  no operation moved by 1% of the time
where the time goes in v4:
time: 130 us
  Pallas kernels  129 us (99%)
  local copies, waits for them, and re-layouts  1.57 us (1%)
    pallas_call x1, Pallas kernels, on_device(): pl.pallas_call(functools.partial(kernel, n_ep, n_tp, cap), out_shape=jax....  129 us

profile of v4, /device:TPU:65, one launch (start us, length us, event | category | flops | bytes accessed | tf_op | source)
XLA Modules:
  0.0 130.3 jit_solution(15869871661928122226)
XLA Ops:
  0.0 128.7 %shard_map.73 = bf16[256,256]{1,0:T(8,128)(2,1)} custom-call(bf16[256,256]{1,0:T(8,128)(2,1)} %tok_hbm.1, f32[16,128]{1,0:T(8,128)} %bitcast.9, s32[2,256]{1,0:T(2,128)} %bitcast.10, f32[2,256]{1,0:T(2,128)} %bitcast.11, bf16[2048,384]{1,0:T(8,128)(2,1)} %bitcast.6, bf16[2048,384]{1,0:T(8,128)(2,1)} %bitcast.7, bf16[384,2048]{1,0:T(8,128)(2,1)} %bitcast.8), custom_call_target="tpu_custom_call" | custom-call | tf_op jit(solution)/shard_map/pallas_call | solution.py:359
  128.8 1.6 %copy.9 = bf16[256,256]{1,0:T(8,128)(2,1)} copy(bf16[256,256]{1,0:T(8,128)(2,1)} %shard_map.73) | data formatting | bytes 262144
